TPU v7x, 256 devices: a whole 4x4x8 slice. The times are simulated.
256 devices in a mesh: sp: 32 (over z, y), tp: 8 (over x, core).
Axes of the slice: x: 4, y: 4, z: 8, core: 2. Of those that a mesh axis runs over, the one named last changes fastest.
Arguments:
- residual_in: bfloat16 [12288, 2048], P(('sp', 'tp')), may hold values from -6 to 6
- queries: bfloat16 [12288, 2048], P('sp', 'tp'), may hold values from -180 to 180
- keys: bfloat16 [12288, 2048], P('sp', 'tp'), may hold values from -9 to 9
- values: bfloat16 [12288, 2048], P('sp', 'tp'), may hold values from -6 to 6
- mix_lambda: float32 [16], P('tp'), may hold values from 0.3 to 0.8
- head_gain: float32 [128], replicated, may hold values from 0.1 to 1.9
- out_weight: bfloat16 [2048, 2048], P('tp'), may hold values from -0.125 to 0.125
- norm_gain: float32 [2048], replicated, may hold values from 0.1 to 1.9
- gate_weight: bfloat16 [2048, 5632], P('sp', 'tp'), may hold values from -0.125 to 0.125
- up_weight: bfloat16 [2048, 5632], P('sp', 'tp'), may hold values from -0.125 to 0.125
- down_weight: bfloat16 [5632, 2048], P('tp', 'sp'), may hold values from -0.078125 to 0.078125
Outputs:
- layer_out: bfloat16 [12288, 2048], P(('sp', 'tp'))
All inputs are finite; a program needn't handle non-finite values.
Results may differ from a plain program's by a relative error of at most 0.014.
Values may be sent and summed in bfloat16 or wider, within the bound.
No kernel may reach another device: no remote copies, remote signals or barrier semaphores. Data moves between devices by JAX's collectives and lax.ppermute only.
A program may use at most 128 MiB of HBM per device.

v0:
```python
import math
import jax
import jax.numpy as jnp
from jax import lax
from jax.sharding import PartitionSpec as P

DH = 64
VD = 128


def cut_along(value, dim, devices):
    shape = value.shape
    parts = value.reshape(*shape[:dim], devices, shape[dim] // devices, *shape[dim + 1 :])
    return jnp.moveaxis(parts, dim, 0)


def sent_and_summed(value, axis, dim):
    parts = cut_along(value, dim, lax.axis_size(axis))
    arrived = lax.all_to_all(parts, axis, split_axis=0, concat_axis=0, tiled=True)
    return arrived.astype(jnp.float32).sum(axis=0)


def sent_to_all(value, axis):
    copies = jnp.broadcast_to(value, (lax.axis_size(axis), *value.shape))
    return lax.all_to_all(copies, axis, split_axis=0, concat_axis=0, tiled=True)


def joined_along(parts, dim):
    shape = list(parts.shape[1:])
    shape[dim] *= parts.shape[0]
    return jnp.moveaxis(parts, 0, dim).reshape(shape)


def collect(value, axis, dim):
    parts = sent_to_all(value, axis)
    return joined_along(parts, dim)


def rows_first(arrays, axis, dims):
    turned = [jnp.moveaxis(a, dim, 0) for a, dim in zip(arrays, dims)]
    widths = [t[0].size for t in turned]
    both = jnp.concatenate([t.reshape(-1, w) for t, w in zip(turned, widths)], axis=1)
    result = lax.all_gather(both, axis, axis=0, tiled=True)
    parts = jnp.split(result, [sum(widths[:k]) for k in range(1, len(widths))], axis=1)
    return tuple(
        (
            jnp.moveaxis(b.reshape(-1, *t.shape[1:]), 0, dim)
            for b, t, dim in zip(parts, turned, dims)
        )
    )


def body(
    residual_in,
    queries,
    keys,
    values,
    mix_lambda,
    head_gain,
    out_weight,
    norm_gain,
    gate_weight,
    up_weight,
    down_weight,
):
    tok_local = queries.shape[0]
    heads_local = mix_lambda.shape[0]
    query_four = queries.reshape(tok_local, heads_local, 2, DH)
    inverse_root = 1.0 / math.sqrt(DH)

    def one_block(state, block):
        top, total, weighted = state
        key_block, value_block = block
        scores = (
            jnp.einsum("qhcd,khcd->hcqk", query_four, key_block, preferred_element_type=jnp.float32)
            * inverse_root
        )
        new_top = jnp.maximum(top, jnp.max(scores, axis=-1))
        rescale = jnp.exp(top - new_top)
        expo = jnp.exp(scores - new_top[..., None])
        total = total * rescale + jnp.sum(expo, axis=-1)
        weighted = weighted * rescale[..., None] + jnp.einsum(
            "hcqk,khe->hcqe",
            expo.astype(jnp.bfloat16),
            value_block,
            preferred_element_type=jnp.float32,
        )
        return ((new_top, total, weighted), None)

    start_state = (
        jnp.full((heads_local, 2, tok_local), -1e30, jnp.float32),
        jnp.zeros((heads_local, 2, tok_local), jnp.float32),
        jnp.zeros((heads_local, 2, tok_local, VD), jnp.float32),
    )
    key_piece = lax.all_gather(keys, "sp", axis=0, tiled=True)
    value_piece = lax.all_gather(values, "sp", axis=0, tiled=True)
    count = key_piece.shape[0]
    shards = max(count // tok_local, 1)
    unit = count // shards
    group = max(
        (g for g in range(1, shards + 1) if shards % g == 0 and g * unit <= max(1536, unit))
    )
    width = group * unit
    blocks = count // width
    key_blocks = key_piece.reshape(blocks, width, heads_local, 2, DH)
    value_blocks = value_piece.reshape(blocks, width, heads_local, VD)
    state, unused = lax.scan(one_block, start_state, (key_blocks, value_blocks))
    top, total, weighted = state
    maps = weighted / total[..., None]
    mixed = maps[:, 0] - mix_lambda[:, None, None] * maps[:, 1]
    head_scale = lax.rsqrt(jnp.mean(mixed * mixed, axis=-1, keepdims=True) + 1e-06)
    head_out = (mixed * head_scale * head_gain).astype(jnp.bfloat16)
    attended = jnp.transpose(head_out, (1, 0, 2)).reshape(tok_local, heads_local * VD)
    picked = attended
    projected = sent_and_summed(
        jnp.dot(picked, out_weight, preferred_element_type=jnp.float32).astype(jnp.bfloat16),
        "tp",
        0,
    )
    after_mix = residual_in.astype(jnp.float32) + projected
    row_scale = lax.rsqrt(jnp.mean(after_mix * after_mix, axis=-1, keepdims=True) + 1e-06)
    normed = (after_mix * row_scale * norm_gain).astype(jnp.bfloat16)
    all_rows = collect(normed, "tp", 0)
    gate_all, up_all, down_all = rows_first((gate_weight, up_weight, down_weight), "sp", (0, 0, 1))
    gate = jnp.dot(all_rows, gate_all, preferred_element_type=jnp.float32)
    up = jnp.dot(all_rows, up_all, preferred_element_type=jnp.float32)
    hidden = (jax.nn.silu(gate) * up).astype(jnp.bfloat16)
    picked = hidden
    mixer = sent_and_summed(
        jnp.dot(picked, down_all, preferred_element_type=jnp.float32).astype(jnp.bfloat16), "tp", 0
    )
    return (after_mix + 0.5 * mixer).astype(jnp.bfloat16)


def solution(mesh):
    return jax.shard_map(
        body,
        mesh=mesh,
        in_specs=(
            P(("sp", "tp"), None),
            P("sp", "tp"),
            P("sp", "tp"),
            P("sp", "tp"),
            P("tp"),
            P(),
            P("tp", None),
            P(),
            P("sp", "tp"),
            P("sp", "tp"),
            P("tp", "sp"),
        ),
        out_specs=P(("sp", "tp"), None),
        check_vma=False,
    )
```

profile of v0, /device:TPU:1, one launch (start us, length us, event | category | flops | bytes accessed | tf_op | source)
XLA Modules:
  0.0 425.4 jit_solution(3736161622382868444)
XLA Ops:
  11.1 89.9 %all-gather.4.cloned.1.call-done = bf16[12288,256]{1,0:T(8,128)(2,1)} async-done(((bf16[384,256]{1,0:T(8,128)(2,1)}), bf16[12288,256]{1,0:T(8,128)(2,1)}) %all-gather.4.cloned.1.call-update) | async-done | bytes 6291472 | tf_op jit(solution)/shard_map/all_gather | solution.py:95
  101.0 21.8 %reshape.51 = bf16[8,1536,2,2,64]{4,3,2,1,0:T(2,128)(2,1)} reshape(bf16[12288,256]{1,0:T(8,128)(2,1)} %all-gather.4.cloned.1.call-done) | data formatting | bytes 12582912 | tf_op jit(solution)/shard_map/reshape | solution.py:105
  122.8 29.8 %copy.19 = bf16[8,1536,2,2,64]{1,4,3,2,0:T(8,128)(2,1)} copy(bf16[8,1536,2,2,64]{4,3,2,1,0:T(2,128)(2,1)} %reshape.51) | data formatting | bytes 12582912
  152.6 36.1 %all-gather.6.cloned.1.call-done = bf16[12288,256]{1,0:T(8,128)(2,1)} async-done(((bf16[384,256]{1,0:T(8,128)(2,1)}), bf16[12288,256]{1,0:T(8,128)(2,1)}) %all-gather.6.cloned.1.call-update) | async-done | bytes 6291472 | tf_op jit(solution)/shard_map/all_gather | solution.py:96
  188.7 9.7 %reshape.52 = bf16[8,1536,2,128]{3,2,1,0:T(2,128)(2,1)} reshape(bf16[12288,256]{1,0:T(8,128)(2,1)} %all-gather.6.cloned.1.call-done) | data formatting | bytes 12582912 | tf_op jit(solution)/shard_map/reshape | solution.py:106
  198.5 128.2 %while.15 = (s32[]{:T(128)}, f32[2,2,384]{2,1,0:T(2,128)S(1)}, f32[2,2,384]{2,1,0:T(2,128)S(1)}, f32[2,2,384,128]{3,2,1,0:T(8,128)S(1)}, bf16[8,1536,2,2,64]{1,4...) while((s32[]{:T(128)}, f32[2,2,384]{2,1,0:T(2,128)S(1)}, ...), condition=%wide.region_3.4_spmd.clone, body=%wide.region_0.3_spmd.clone.sunk | while | flops 925441536 | bytes 71074440 | solution.py:107
  198.5 6.2 %bitcast_reduce_fusion.2 = (f32[2,2,384]{2,1,0:T(2,128)S(1)}, f32[2,2,1536,384]{3,2,1,0:T(8,128)}) fusion(bf16[384,2,2,64]{0,3,2,1:T(8,128)(2,1)S(1)} %get-tuple-element.168, bf16[8,1536,2,2,64]{1,4,3,2,0:T(8,128)(2,1)} %get-tuple-element.167, s32[]{:T(128)} %get-tuple-element.154), kind=kOutput, calls=%fused_computation.1.clone.1 | convolution fusion | flops 306706944 | bytes 10426880 | tf_op jit(solution)/shard_map/while/body/eval_jaxpr/qhcd,khcd->hcqk/dot_general | solution.py:75
  204.7 5.4 %fusion.55 = f32[2,2,384]{2,1,0:T(2,128)S(1)} fusion(f32[2,2,1536,384]{3,2,1,0:T(8,128)} %get-tuple-element.142, f32[2,2,384]{2,1,0:T(2,128)S(1)} %fusion.54), kind=kLoop, calls=%fused_computation.4.clone.1 | loop fusion | flops 7076352 | bytes 9449472 | tf_op jit(solution)/shard_map/while/body/eval_jaxpr/reduce_sum | solution.py:81
  214.4 6.2 %bitcast_reduce_fusion.2 = (f32[2,2,384]{2,1,0:T(2,128)S(1)}, f32[2,2,1536,384]{3,2,1,0:T(8,128)}) fusion(bf16[384,2,2,64]{0,3,2,1:T(8,128)(2,1)S(1)} %get-tuple-element.168, bf16[8,1536,2,2,64]{1,4,3,2,0:T(8,128)(2,1)} %get-tuple-element.167, s32[]{:T(128)} %get-tuple-element.154), kind=kOutput, calls=%fused_computation.1.clone.1 | convolution fusion | flops 306706944 | bytes 10426880 | tf_op jit(solution)/shard_map/while/body/eval_jaxpr/qhcd,khcd->hcqk/dot_general | solution.py:75
  220.7 5.4 %fusion.55 = f32[2,2,384]{2,1,0:T(2,128)S(1)} fusion(f32[2,2,1536,384]{3,2,1,0:T(8,128)} %get-tuple-element.142, f32[2,2,384]{2,1,0:T(2,128)S(1)} %fusion.54), kind=kLoop, calls=%fused_computation.4.clone.1 | loop fusion | flops 7076352 | bytes 9449472 | tf_op jit(solution)/shard_map/while/body/eval_jaxpr/reduce_sum | solution.py:81
  230.4 6.2 %bitcast_reduce_fusion.2 = (f32[2,2,384]{2,1,0:T(2,128)S(1)}, f32[2,2,1536,384]{3,2,1,0:T(8,128)}) fusion(bf16[384,2,2,64]{0,3,2,1:T(8,128)(2,1)S(1)} %get-tuple-element.168, bf16[8,1536,2,2,64]{1,4,3,2,0:T(8,128)(2,1)} %get-tuple-element.167, s32[]{:T(128)} %get-tuple-element.154), kind=kOutput, calls=%fused_computation.1.clone.1 | convolution fusion | flops 306706944 | bytes 10426880 | tf_op jit(solution)/shard_map/while/body/eval_jaxpr/qhcd,khcd->hcqk/dot_general | solution.py:75
  236.6 5.6 %fusion.55 = f32[2,2,384]{2,1,0:T(2,128)S(1)} fusion(f32[2,2,1536,384]{3,2,1,0:T(8,128)} %get-tuple-element.142, f32[2,2,384]{2,1,0:T(2,128)S(1)} %fusion.54), kind=kLoop, calls=%fused_computation.4.clone.1 | loop fusion | flops 7076352 | bytes 9449472 | tf_op jit(solution)/shard_map/while/body/eval_jaxpr/reduce_sum | solution.py:81
  246.8 6.2 %bitcast_reduce_fusion.2 = (f32[2,2,384]{2,1,0:T(2,128)S(1)}, f32[2,2,1536,384]{3,2,1,0:T(8,128)}) fusion(bf16[384,2,2,64]{0,3,2,1:T(8,128)(2,1)S(1)} %get-tuple-element.168, bf16[8,1536,2,2,64]{1,4,3,2,0:T(8,128)(2,1)} %get-tuple-element.167, s32[]{:T(128)} %get-tuple-element.154), kind=kOutput, calls=%fused_computation.1.clone.1 | convolution fusion | flops 306706944 | bytes 10426880 | tf_op jit(solution)/shard_map/while/body/eval_jaxpr/qhcd,khcd->hcqk/dot_general | solution.py:75
  253.0 5.6 %fusion.55 = f32[2,2,384]{2,1,0:T(2,128)S(1)} fusion(f32[2,2,1536,384]{3,2,1,0:T(8,128)} %get-tuple-element.142, f32[2,2,384]{2,1,0:T(2,128)S(1)} %fusion.54), kind=kLoop, calls=%fused_computation.4.clone.1 | loop fusion | flops 7076352 | bytes 9449472 | tf_op jit(solution)/shard_map/while/body/eval_jaxpr/reduce_sum | solution.py:81
  263.0 6.2 %bitcast_reduce_fusion.2 = (f32[2,2,384]{2,1,0:T(2,128)S(1)}, f32[2,2,1536,384]{3,2,1,0:T(8,128)}) fusion(bf16[384,2,2,64]{0,3,2,1:T(8,128)(2,1)S(1)} %get-tuple-element.168, bf16[8,1536,2,2,64]{1,4,3,2,0:T(8,128)(2,1)} %get-tuple-element.167, s32[]{:T(128)} %get-tuple-element.154), kind=kOutput, calls=%fused_computation.1.clone.1 | convolution fusion | flops 306706944 | bytes 10426880 | tf_op jit(solution)/shard_map/while/body/eval_jaxpr/qhcd,khcd->hcqk/dot_general | solution.py:75
  269.2 5.4 %fusion.55 = f32[2,2,384]{2,1,0:T(2,128)S(1)} fusion(f32[2,2,1536,384]{3,2,1,0:T(8,128)} %get-tuple-element.142, f32[2,2,384]{2,1,0:T(2,128)S(1)} %fusion.54), kind=kLoop, calls=%fused_computation.4.clone.1 | loop fusion | flops 7076352 | bytes 9449472 | tf_op jit(solution)/shard_map/while/body/eval_jaxpr/reduce_sum | solution.py:81
  279.0 6.2 %bitcast_reduce_fusion.2 = (f32[2,2,384]{2,1,0:T(2,128)S(1)}, f32[2,2,1536,384]{3,2,1,0:T(8,128)}) fusion(bf16[384,2,2,64]{0,3,2,1:T(8,128)(2,1)S(1)} %get-tuple-element.168, bf16[8,1536,2,2,64]{1,4,3,2,0:T(8,128)(2,1)} %get-tuple-element.167, s32[]{:T(128)} %get-tuple-element.154), kind=kOutput, calls=%fused_computation.1.clone.1 | convolution fusion | flops 306706944 | bytes 10426880 | tf_op jit(solution)/shard_map/while/body/eval_jaxpr/qhcd,khcd->hcqk/dot_general | solution.py:75
  285.2 5.4 %fusion.55 = f32[2,2,384]{2,1,0:T(2,128)S(1)} fusion(f32[2,2,1536,384]{3,2,1,0:T(8,128)} %get-tuple-element.142, f32[2,2,384]{2,1,0:T(2,128)S(1)} %fusion.54), kind=kLoop, calls=%fused_computation.4.clone.1 | loop fusion | flops 7076352 | bytes 9449472 | tf_op jit(solution)/shard_map/while/body/eval_jaxpr/reduce_sum | solution.py:81
  294.9 6.2 %bitcast_reduce_fusion.2 = (f32[2,2,384]{2,1,0:T(2,128)S(1)}, f32[2,2,1536,384]{3,2,1,0:T(8,128)}) fusion(bf16[384,2,2,64]{0,3,2,1:T(8,128)(2,1)S(1)} %get-tuple-element.168, bf16[8,1536,2,2,64]{1,4,3,2,0:T(8,128)(2,1)} %get-tuple-element.167, s32[]{:T(128)} %get-tuple-element.154), kind=kOutput, calls=%fused_computation.1.clone.1 | convolution fusion | flops 306706944 | bytes 10426880 | tf_op jit(solution)/shard_map/while/body/eval_jaxpr/qhcd,khcd->hcqk/dot_general | solution.py:75
  310.8 6.2 %bitcast_reduce_fusion.2 = (f32[2,2,384]{2,1,0:T(2,128)S(1)}, f32[2,2,1536,384]{3,2,1,0:T(8,128)}) fusion(bf16[384,2,2,64]{0,3,2,1:T(8,128)(2,1)S(1)} %get-tuple-element.168, bf16[8,1536,2,2,64]{1,4,3,2,0:T(8,128)(2,1)} %get-tuple-element.167, s32[]{:T(128)} %get-tuple-element.154), kind=kOutput, calls=%fused_computation.1.clone.1 | convolution fusion | flops 306706944 | bytes 10426880 | tf_op jit(solution)/shard_map/while/body/eval_jaxpr/qhcd,khcd->hcqk/dot_general | solution.py:75
  328.3 26.4 %all_to_all.15 = bf16[8,48,2048]{2,1,0:T(8,128)(2,1)S(1)} all-to-all(bf16[8,48,2048]{2,1,0:T(8,128)(2,1)S(1)} %bitcast.67), channel_id=1, replica_groups=mesh['sp'=32,'tp'=8] {'tp'}, dimensions={0} | all-to-all | bytes 3145728 | tf_op jit(solution)/shard_map/all_to_all | solution.py:19
  355.4 24.0 %all_to_all.16 = bf16[8,48,2048]{2,1,0:T(8,128)(2,1)S(1)} all-to-all(bf16[8,48,2048]{2,1,0:T(8,128)(2,1)S(1)} %broadcast_in_dim.13), channel_id=1, replica_groups=mesh['sp'=32,'tp'=8] {'tp'}, dimensions={0} | all-to-all | bytes 3145728 | tf_op jit(solution)/shard_map/all_to_all | solution.py:25
  384.0 8.8 %fusion.23 = bf16[384,2048]{1,0:T(8,128)(2,1)} fusion(bf16[2048,2112]{1,0:T(8,128)(2,1)} %all-gather.8.cloned.1.call-done, bf16[384,2048]{1,0:T(8,128)(2,1)S(1)} %bitcast.69, f32[384,704]{0,1:T(8,128)} %fusion.21), kind=kOutput, calls=%fused_computation.30 | convolution fusion | flops 2217000960 | bytes 10518528 | tf_op jit(solution)/shard_map/dot_general | solution.py:130
  392.8 25.1 %all_to_all.17 = bf16[8,48,2048]{2,1,0:T(8,128)(2,1)S(1)} all-to-all(bf16[8,48,2048]{2,1,0:T(8,128)(2,1)} %bitcast.70), channel_id=1, replica_groups=mesh['sp'=32,'tp'=8] {'tp'}, dimensions={0} | all-to-all | bytes 3145728 | tf_op jit(solution)/shard_map/all_to_all | solution.py:19
  (95 shorter events, 57.5 us)
Async XLA Ops:
  6.5 321.1 %copy-start = (bf16[256,2048]{1,0:T(8,128)(2,1)S(1)}, bf16[256,2048]{1,0:T(8,128)(2,1)}, u32[]{:S(2)}) copy-start(bf16[256,2048]{1,0:T(8,128)(2,1)} %param.19) | copy-start | bytes 3145732
  6.5 94.5 %all-gather.4.cloned.1.call-start = ((), (), s32[]{:S(2)}) async-start(), calls=%async_computation.3 | async-start | bytes 6488064 | tf_op jit(solution)/shard_map/all_gather | solution.py:95
  7.3 181.5 %all-gather.6.cloned.1.call-start = ((), (), s32[]{:S(2)}) async-start(), calls=%async_computation.4 | async-start | bytes 6488064 | tf_op jit(solution)/shard_map/all_gather | solution.py:96
  8.0 371.5 %all-gather.8.cloned.1.call-start = ((), (), s32[]{:S(2)}) async-start(), calls=%async_computation.5 | async-start | bytes 9191424 | tf_op jit(solution)/shard_map/all_gather | solution.py:43
  204.7 7.1 %copy-start.1 = (f32[2,2,1536,384]{3,2,1,0:T(8,128)S(1)}, f32[2,2,1536,384]{3,2,1,0:T(8,128)}, u32[]{:S(2)}) copy-start(f32[2,2,1536,384]{3,2,1,0:T(8,128)} %get-tuple-element.142) | copy-start | bytes 28311556 | tf_op jit(solution)/shard_map/while
  220.7 7.1 %copy-start.1 = (f32[2,2,1536,384]{3,2,1,0:T(8,128)S(1)}, f32[2,2,1536,384]{3,2,1,0:T(8,128)}, u32[]{:S(2)}) copy-start(f32[2,2,1536,384]{3,2,1,0:T(8,128)} %get-tuple-element.142) | copy-start | bytes 28311556 | tf_op jit(solution)/shard_map/while
  236.6 7.5 %copy-start.1 = (f32[2,2,1536,384]{3,2,1,0:T(8,128)S(1)}, f32[2,2,1536,384]{3,2,1,0:T(8,128)}, u32[]{:S(2)}) copy-start(f32[2,2,1536,384]{3,2,1,0:T(8,128)} %get-tuple-element.142) | copy-start | bytes 28311556 | tf_op jit(solution)/shard_map/while
  253.0 7.3 %copy-start.1 = (f32[2,2,1536,384]{3,2,1,0:T(8,128)S(1)}, f32[2,2,1536,384]{3,2,1,0:T(8,128)}, u32[]{:S(2)}) copy-start(f32[2,2,1536,384]{3,2,1,0:T(8,128)} %get-tuple-element.142) | copy-start | bytes 28311556 | tf_op jit(solution)/shard_map/while
  269.2 7.1 %copy-start.1 = (f32[2,2,1536,384]{3,2,1,0:T(8,128)S(1)}, f32[2,2,1536,384]{3,2,1,0:T(8,128)}, u32[]{:S(2)}) copy-start(f32[2,2,1536,384]{3,2,1,0:T(8,128)} %get-tuple-element.142) | copy-start | bytes 28311556 | tf_op jit(solution)/shard_map/while
  285.2 7.0 %copy-start.1 = (f32[2,2,1536,384]{3,2,1,0:T(8,128)S(1)}, f32[2,2,1536,384]{3,2,1,0:T(8,128)}, u32[]{:S(2)}) copy-start(f32[2,2,1536,384]{3,2,1,0:T(8,128)} %get-tuple-element.142) | copy-start | bytes 28311556 | tf_op jit(solution)/shard_map/while
  301.1 7.0 %copy-start.1 = (f32[2,2,1536,384]{3,2,1,0:T(8,128)S(1)}, f32[2,2,1536,384]{3,2,1,0:T(8,128)}, u32[]{:S(2)}) copy-start(f32[2,2,1536,384]{3,2,1,0:T(8,128)} %get-tuple-element.142) | copy-start | bytes 28311556 | tf_op jit(solution)/shard_map/while
  317.0 7.0 %copy-start.1 = (f32[2,2,1536,384]{3,2,1,0:T(8,128)S(1)}, f32[2,2,1536,384]{3,2,1,0:T(8,128)}, u32[]{:S(2)}) copy-start(f32[2,2,1536,384]{3,2,1,0:T(8,128)} %get-tuple-element.142) | copy-start | bytes 28311556 | tf_op jit(solution)/shard_map/while
  326.7 0.7 copy-start.4
  326.7 0.8 copy-start.5
  328.3 26.7 %copy-start.2 = (bf16[48,2048]{1,0:T(8,128)(2,1)S(1)}, bf16[48,2048]{1,0:T(8,128)(2,1)}, u32[]{:S(2)}) copy-start(bf16[48,2048]{1,0:T(8,128)(2,1)} %param.13) | copy-start | bytes 589828
  328.3 26.8 %copy-start.3 = (f32[2048]{0:T(1024)S(1)}, f32[2048]{0:T(1024)}, u32[]{:S(2)}) copy-start(f32[2048]{0:T(1024)} %param.20) | copy-start | bytes 24580
Sparse Core Ops, SparseCore 0:
  9.9 91.0 all-gather.3
  103.6 85.0 all-gather.5
  191.3 97.5 all-gather.7
where the time goes:
time: 428 us; the launch traced here: 425 us
  waiting for transfers between devices  127 us (30%)
  matrix products  84.7 us (20%)
  local copies, waits for them, and re-layouts  78.1 us (18%)
  blocking collectives  75.5 us (18%)
  other arithmetic  45.7 us (11%)
  between operations  13.3 us (3%)
    all_gather x1, waiting for transfers between devices, body(): key_piece = lax.all_gather(keys, 'sp', axis=0, tiled=True)  89.9 us
    all_to_all x2, blocking collectives, sent_and_summed(): lax.all_to_all(parts, axis, split_axis=0, concat_axis=0, tiled=True)  51.5 us
    dot_general x8, matrix products, one_block(): jnp.einsum('qhcd,khcd->hcqk', query_four, key_block, preferred_element_ty...  49.6 us
    reduce_sum x8, other arithmetic, one_block(): total = total * rescale + jnp.sum(expo, axis=-1)  43.7 us
    all_gather x1, waiting for transfers between devices, body(): value_piece = lax.all_gather(values, 'sp', axis=0, tiled=True)  36.1 us
    unnamed x12, local copies, waits for them, and re-layouts  31.2 us
    all_to_all x1, blocking collectives, sent_to_all(): return lax.all_to_all(copies, axis, split_axis=0, concat_axis=0, tiled=True)  24 us
    reshape x1, local copies, waits for them, and re-layouts, body(): key_blocks = key_piece.reshape(blocks, width, heads_local, 2, DH)  21.8 us
  transfers between devices with their start and end apart: 3, of which 2 were waited for; matrix products, arithmetic and copies ran while one was open for 46% of the time, Pallas kernels for 0%

commit v1 on v0

--- a/solution.py
+++ b/solution.py
@@ -3,6 +3,7 @@
 import jax.numpy as jnp
 from jax import lax
 from jax.sharding import PartitionSpec as P
+from jax.lax import all_to_all, axis_size
 
 DH = 64
 VD = 128
@@ -92,7 +93,10 @@
         jnp.zeros((heads_local, 2, tok_local), jnp.float32),
         jnp.zeros((heads_local, 2, tok_local, VD), jnp.float32),
     )
-    key_piece = lax.all_gather(keys, "sp", axis=0, tiled=True)
+    time_the_rounds = lambda patch: jnp.concatenate(
+        all_to_all(jnp.stack(axis_size("sp") * [patch]), "sp", 0, 0), axis=0
+    )
+    key_piece = time_the_rounds(keys)
     value_piece = lax.all_gather(values, "sp", axis=0, tiled=True)
     count = key_piece.shape[0]
     shards = max(count // tok_local, 1)

time: 428 us -> 465 us (1.086)
  waiting for transfers between devices: 127 us -> 173 us
  local copies, waits for them, and re-layouts: 78.1 us -> 56.6 us
  starting transfers between devices: 0.08 us -> 12.3 us
    all_to_all x0 -> x1, waiting for transfers between devices: none -> 173 us  [body(): all_to_all(jnp.stack(axis_size('sp') * [patch]), 'sp', 0, 0)]
    all_gather x1 -> x0, waiting for transfers between devices: 89.9 us -> none  [body(): key_piece = lax.all_gather(keys, 'sp', axis=0, tiled=True)]
    all_gather x1, waiting for transfers between devices: 36.1 us -> 0.01 us  [body(): value_piece = lax.all_gather(values, 'sp', axis=0, tiled=True)]
    unnamed x12 -> x21, local copies, waits for them, and re-layouts: 31.2 us -> 9.01 us
    reshape x1 -> x0, local copies, waits for them, and re-layouts: 21.8 us -> none  [body(): key_blocks = key_piece.reshape(blocks, width, heads_local, 2, DH)]
    another operation x0 -> x2, local copies, waits for them, and re-layouts: none -> 14.4 us  [the longest x1 10.7 us: body(): key_blocks = key_piece.reshape(blocks, width, heads_local, 2, DH)]
    all_to_all x0 -> x1, starting transfers between devices: none -> 12.3 us  [body(): all_to_all(jnp.stack(axis_size('sp') * [patch]), 'sp', 0, 0)]
    all_to_all x0 -> x1, local copies, waits for them, and re-layouts: none -> 9.22 us  [body(): all_to_all(jnp.stack(axis_size('sp') * [patch]), 'sp', 0, 0)]
  transfers between devices with their start and end apart: 3 -> 3, of which waited for: 2 -> 1; matrix products, arithmetic and copies ran while one was open for 46% -> 37% of each run, Pallas kernels for 0% -> 0%
where the time goes in v1:
time: 465 us; the launch traced here: 464 us
  waiting for transfers between devices  173 us (37%)
  matrix products  84.6 us (18%)
  blocking collectives  77 us (17%)
  local copies, waits for them, and re-layouts  56.6 us (12%)
  other arithmetic  45.6 us (10%)
  between operations  13.6 us (3%)
  starting transfers between devices  12.3 us (3%)
    all_to_all x1, waiting for transfers between devices, body(): all_to_all(jnp.stack(axis_size('sp') * [patch]), 'sp', 0, 0)  173 us
    all_to_all x2, blocking collectives, sent_and_summed(): lax.all_to_all(parts, axis, split_axis=0, concat_axis=0, tiled=True)  53 us
    dot_general x8, matrix products, one_block(): jnp.einsum('qhcd,khcd->hcqk', query_four, key_block, preferred_element_ty...  49.6 us
    reduce_sum x8, other arithmetic, one_block(): total = total * rescale + jnp.sum(expo, axis=-1)  43.5 us
    all_to_all x1, blocking collectives, sent_to_all(): return lax.all_to_all(copies, axis, split_axis=0, concat_axis=0, tiled=True)  24 us
    dot_general x8, matrix products, one_block(): jnp.einsum('hcqk,khe->hcqe', expo.astype(jnp.bfloat16), value_block, pref...  21.2 us
    dynamic_slice x8, local copies, waits for them, and re-layouts, body(): state, unused = lax.scan(one_block, start_state, (key_blocks, value_blocks))  12.9 us
    all_to_all x1, starting transfers between devices, body(): all_to_all(jnp.stack(axis_size('sp') * [patch]), 'sp', 0, 0)  12.3 us
  transfers between devices with their start and end apart: 3, of which 1 were waited for; matrix products, arithmetic and copies ran while one was open for 37% of the time, Pallas kernels for 0%

profile of v1, /device:TPU:1, one launch (start us, length us, event | category | flops | bytes accessed | tf_op | source)
XLA Modules:
  0.0 463.6 jit_solution(5589878337944765438)
XLA Ops:
  12.0 12.3 %all-to-all-start = ((bf16[32,384,256]{1,2,0:T(8,128)(2,1)}), bf16[32,384,256]{1,2,0:T(8,128)(2,1)}, u32[]{:S(2)}, u32[]{:S(2)}) async-start(bf16[32,384,256]{1,2,0:T(8,128)(2,1)} %stack.2), calls=%async_computation | async-start | bytes 12582912 | tf_op jit(solution)/shard_map/all_to_all | solution.py:97
  25.5 172.5 %all-to-all-done = bf16[32,384,256]{1,2,0:T(8,128)(2,1)} async-done(((bf16[32,384,256]{1,2,0:T(8,128)(2,1)}), bf16[32,384,256]{1,2,0:T(8,128)(2,1)}, u32[]{:S(2)}, u32[]{:S(2)}) %all-to-all-start) | async-done | bytes 6291488 | tf_op jit(solution)/shard_map/all_to_all | solution.py:97
  198.0 9.2 %copy.25 = bf16[32,384,256]{1,0,2:T(8,128)(2,1)} copy(bf16[32,384,256]{1,2,0:T(8,128)(2,1)} %all-to-all-done) | data formatting | bytes 12582912 | tf_op jit(solution)/shard_map/all_to_all | solution.py:97
  207.2 10.7 %reshape_reshape.3 = bf16[8,1536,2,2,64]{1,0,4,3,2:T(8,128)(2,1)} reshape(bf16[32,384,256]{1,0,2:T(8,128)(2,1)} %copy.25) | data formatting | bytes 12582912 | tf_op jit(solution)/shard_map/reshape;reshape | solution.py:109
  217.9 7.4 %copy.28 = bf16[8,1536,2,2,64]{1,4,3,2,0:T(8,128)(2,1)} copy(bf16[8,1536,2,2,64]{1,0,4,3,2:T(8,128)(2,1)} %reshape_reshape.3) | data formatting | bytes 12582912
  225.4 9.8 %reshape.49 = bf16[8,1536,2,128]{3,2,1,0:T(2,128)(2,1)} reshape(bf16[12288,256]{1,0:T(8,128)(2,1)} %all-gather.3.cloned.1.call-done) | data formatting | bytes 12582912 | tf_op jit(solution)/shard_map/reshape | solution.py:110
  235.1 128.0 %while.15 = (s32[]{:T(128)}, f32[2,2,384]{2,1,0:T(2,128)S(1)}, f32[2,2,384]{2,1,0:T(2,128)S(1)}, f32[2,2,384,128]{3,2,1,0:T(8,128)S(1)}, bf16[8,1536,2,2,64]{1,4...) while((s32[]{:T(128)}, f32[2,2,384]{2,1,0:T(2,128)S(1)}, ...), condition=%wide.region_3.4_spmd.clone, body=%wide.region_0.3_spmd.clone.sunk | while | flops 925441536 | bytes 71074440 | solution.py:111
  235.1 6.2 %bitcast_reduce_fusion.2 = (f32[2,2,384]{2,1,0:T(2,128)S(1)}, f32[2,2,1536,384]{3,2,1,0:T(8,128)}) fusion(bf16[384,2,2,64]{0,3,2,1:T(8,128)(2,1)S(1)} %get-tuple-element.175, bf16[8,1536,2,2,64]{1,4,3,2,0:T(8,128)(2,1)} %get-tuple-element.174, s32[]{:T(128)} %get-tuple-element.161), kind=kOutput, calls=%fused_computation.1.clone.1 | convolution fusion | flops 306706944 | bytes 10426880 | tf_op jit(solution)/shard_map/while/body/eval_jaxpr/qhcd,khcd->hcqk/dot_general | solution.py:76
  241.4 5.4 %fusion.55 = f32[2,2,384]{2,1,0:T(2,128)S(1)} fusion(f32[2,2,1536,384]{3,2,1,0:T(8,128)} %get-tuple-element.149, f32[2,2,384]{2,1,0:T(2,128)S(1)} %fusion.54), kind=kLoop, calls=%fused_computation.4.clone.1 | loop fusion | flops 7076352 | bytes 9449472 | tf_op jit(solution)/shard_map/while/body/eval_jaxpr/reduce_sum | solution.py:82
  251.0 6.2 %bitcast_reduce_fusion.2 = (f32[2,2,384]{2,1,0:T(2,128)S(1)}, f32[2,2,1536,384]{3,2,1,0:T(8,128)}) fusion(bf16[384,2,2,64]{0,3,2,1:T(8,128)(2,1)S(1)} %get-tuple-element.175, bf16[8,1536,2,2,64]{1,4,3,2,0:T(8,128)(2,1)} %get-tuple-element.174, s32[]{:T(128)} %get-tuple-element.161), kind=kOutput, calls=%fused_computation.1.clone.1 | convolution fusion | flops 306706944 | bytes 10426880 | tf_op jit(solution)/shard_map/while/body/eval_jaxpr/qhcd,khcd->hcqk/dot_general | solution.py:76
  257.3 5.5 %fusion.55 = f32[2,2,384]{2,1,0:T(2,128)S(1)} fusion(f32[2,2,1536,384]{3,2,1,0:T(8,128)} %get-tuple-element.149, f32[2,2,384]{2,1,0:T(2,128)S(1)} %fusion.54), kind=kLoop, calls=%fused_computation.4.clone.1 | loop fusion | flops 7076352 | bytes 9449472 | tf_op jit(solution)/shard_map/while/body/eval_jaxpr/reduce_sum | solution.py:82
  267.1 6.2 %bitcast_reduce_fusion.2 = (f32[2,2,384]{2,1,0:T(2,128)S(1)}, f32[2,2,1536,384]{3,2,1,0:T(8,128)}) fusion(bf16[384,2,2,64]{0,3,2,1:T(8,128)(2,1)S(1)} %get-tuple-element.175, bf16[8,1536,2,2,64]{1,4,3,2,0:T(8,128)(2,1)} %get-tuple-element.174, s32[]{:T(128)} %get-tuple-element.161), kind=kOutput, calls=%fused_computation.1.clone.1 | convolution fusion | flops 306706944 | bytes 10426880 | tf_op jit(solution)/shard_map/while/body/eval_jaxpr/qhcd,khcd->hcqk/dot_general | solution.py:76
  273.4 5.7 %fusion.55 = f32[2,2,384]{2,1,0:T(2,128)S(1)} fusion(f32[2,2,1536,384]{3,2,1,0:T(8,128)} %get-tuple-element.149, f32[2,2,384]{2,1,0:T(2,128)S(1)} %fusion.54), kind=kLoop, calls=%fused_computation.4.clone.1 | loop fusion | flops 7076352 | bytes 9449472 | tf_op jit(solution)/shard_map/while/body/eval_jaxpr/reduce_sum | solution.py:82
  283.5 6.2 %bitcast_reduce_fusion.2 = (f32[2,2,384]{2,1,0:T(2,128)S(1)}, f32[2,2,1536,384]{3,2,1,0:T(8,128)}) fusion(bf16[384,2,2,64]{0,3,2,1:T(8,128)(2,1)S(1)} %get-tuple-element.175, bf16[8,1536,2,2,64]{1,4,3,2,0:T(8,128)(2,1)} %get-tuple-element.174, s32[]{:T(128)} %get-tuple-element.161), kind=kOutput, calls=%fused_computation.1.clone.1 | convolution fusion | flops 306706944 | bytes 10426880 | tf_op jit(solution)/shard_map/while/body/eval_jaxpr/qhcd,khcd->hcqk/dot_general | solution.py:76
  289.7 5.4 %fusion.55 = f32[2,2,384]{2,1,0:T(2,128)S(1)} fusion(f32[2,2,1536,384]{3,2,1,0:T(8,128)} %get-tuple-element.149, f32[2,2,384]{2,1,0:T(2,128)S(1)} %fusion.54), kind=kLoop, calls=%fused_computation.4.clone.1 | loop fusion | flops 7076352 | bytes 9449472 | tf_op jit(solution)/shard_map/while/body/eval_jaxpr/reduce_sum | solution.py:82
  299.5 6.2 %bitcast_reduce_fusion.2 = (f32[2,2,384]{2,1,0:T(2,128)S(1)}, f32[2,2,1536,384]{3,2,1,0:T(8,128)}) fusion(bf16[384,2,2,64]{0,3,2,1:T(8,128)(2,1)S(1)} %get-tuple-element.175, bf16[8,1536,2,2,64]{1,4,3,2,0:T(8,128)(2,1)} %get-tuple-element.174, s32[]{:T(128)} %get-tuple-element.161), kind=kOutput, calls=%fused_computation.1.clone.1 | convolution fusion | flops 306706944 | bytes 10426880 | tf_op jit(solution)/shard_map/while/body/eval_jaxpr/qhcd,khcd->hcqk/dot_general | solution.py:76
  305.7 5.4 %fusion.55 = f32[2,2,384]{2,1,0:T(2,128)S(1)} fusion(f32[2,2,1536,384]{3,2,1,0:T(8,128)} %get-tuple-element.149, f32[2,2,384]{2,1,0:T(2,128)S(1)} %fusion.54), kind=kLoop, calls=%fused_computation.4.clone.1 | loop fusion | flops 7076352 | bytes 9449472 | tf_op jit(solution)/shard_map/while/body/eval_jaxpr/reduce_sum | solution.py:82
  315.4 6.2 %bitcast_reduce_fusion.2 = (f32[2,2,384]{2,1,0:T(2,128)S(1)}, f32[2,2,1536,384]{3,2,1,0:T(8,128)}) fusion(bf16[384,2,2,64]{0,3,2,1:T(8,128)(2,1)S(1)} %get-tuple-element.175, bf16[8,1536,2,2,64]{1,4,3,2,0:T(8,128)(2,1)} %get-tuple-element.174, s32[]{:T(128)} %get-tuple-element.161), kind=kOutput, calls=%fused_computation.1.clone.1 | convolution fusion | flops 306706944 | bytes 10426880 | tf_op jit(solution)/shard_map/while/body/eval_jaxpr/qhcd,khcd->hcqk/dot_general | solution.py:76
  331.3 6.2 %bitcast_reduce_fusion.2 = (f32[2,2,384]{2,1,0:T(2,128)S(1)}, f32[2,2,1536,384]{3,2,1,0:T(8,128)}) fusion(bf16[384,2,2,64]{0,3,2,1:T(8,128)(2,1)S(1)} %get-tuple-element.175, bf16[8,1536,2,2,64]{1,4,3,2,0:T(8,128)(2,1)} %get-tuple-element.174, s32[]{:T(128)} %get-tuple-element.161), kind=kOutput, calls=%fused_computation.1.clone.1 | convolution fusion | flops 306706944 | bytes 10426880 | tf_op jit(solution)/shard_map/while/body/eval_jaxpr/qhcd,khcd->hcqk/dot_general | solution.py:76
  347.2 6.2 %bitcast_reduce_fusion.2 = (f32[2,2,384]{2,1,0:T(2,128)S(1)}, f32[2,2,1536,384]{3,2,1,0:T(8,128)}) fusion(bf16[384,2,2,64]{0,3,2,1:T(8,128)(2,1)S(1)} %get-tuple-element.175, bf16[8,1536,2,2,64]{1,4,3,2,0:T(8,128)(2,1)} %get-tuple-element.174, s32[]{:T(128)} %get-tuple-element.161), kind=kOutput, calls=%fused_computation.1.clone.1 | convolution fusion | flops 306706944 | bytes 10426880 | tf_op jit(solution)/shard_map/while/body/eval_jaxpr/qhcd,khcd->hcqk/dot_general | solution.py:76
  364.7 27.9 %all_to_all.20 = bf16[8,48,2048]{2,1,0:T(8,128)(2,1)S(1)} all-to-all(bf16[8,48,2048]{2,1,0:T(8,128)(2,1)S(1)} %bitcast.69), channel_id=1, replica_groups=mesh['sp'=32,'tp'=8] {'tp'}, dimensions={0} | all-to-all | bytes 3145728 | tf_op jit(solution)/shard_map/all_to_all | solution.py:20
  393.3 24.0 %all_to_all.21 = bf16[8,48,2048]{2,1,0:T(8,128)(2,1)S(1)} all-to-all(bf16[8,48,2048]{2,1,0:T(8,128)(2,1)S(1)} %broadcast_in_dim.13), channel_id=1, replica_groups=mesh['sp'=32,'tp'=8] {'tp'}, dimensions={0} | all-to-all | bytes 3145728 | tf_op jit(solution)/shard_map/all_to_all | solution.py:26
  421.9 8.7 %fusion.23 = bf16[384,2048]{1,0:T(8,128)(2,1)} fusion(bf16[2048,2112]{1,0:T(8,128)(2,1)} %all-gather.5.cloned.1.call-done, bf16[384,2048]{1,0:T(8,128)(2,1)S(1)} %bitcast.71, f32[384,704]{0,1:T(8,128)} %fusion.21), kind=kOutput, calls=%fused_computation.30 | convolution fusion | flops 2217000960 | bytes 10518528 | tf_op jit(solution)/shard_map/dot_general | solution.py:134
  430.7 25.1 %all_to_all.22 = bf16[8,48,2048]{2,1,0:T(8,128)(2,1)S(1)} all-to-all(bf16[8,48,2048]{2,1,0:T(8,128)(2,1)} %bitcast.72), channel_id=1, replica_groups=mesh['sp'=32,'tp'=8] {'tp'}, dimensions={0} | all-to-all | bytes 3145728 | tf_op jit(solution)/shard_map/all_to_all | solution.py:20
  (105 shorter events, 64.9 us)
Async XLA Ops:
  6.5 357.5 %copy-start = (bf16[256,2048]{1,0:T(8,128)(2,1)S(1)}, bf16[256,2048]{1,0:T(8,128)(2,1)}, u32[]{:S(2)}) copy-start(bf16[256,2048]{1,0:T(8,128)(2,1)} %param.19) | copy-start | bytes 3145732
  6.5 218.8 %all-gather.3.cloned.1.call-start = ((), (), s32[]{:S(2)}) async-start(), calls=%async_computation.4 | async-start | bytes 6488064 | tf_op jit(solution)/shard_map/all_gather | solution.py:100
  12.0 12.4 %copy-start.4 = (bf16[64,704]{1,0:T(8,128)(2,1)S(1)}, bf16[64,704]{1,0:T(8,128)(2,1)}, u32[]{:S(2)}) copy-start(bf16[64,704]{1,0:T(8,128)(2,1)} %param.21) | copy-start | bytes 270340
  12.0 12.4 %copy-start.5 = (bf16[64,704]{1,0:T(8,128)(2,1)S(1)}, bf16[64,704]{1,0:T(8,128)(2,1)}, u32[]{:S(2)}) copy-start(bf16[64,704]{1,0:T(8,128)(2,1)} %param.22) | copy-start | bytes 270340
  12.0 12.4 %copy-start.6 = (bf16[704,64]{0,1:T(8,128)(2,1)S(1)}, bf16[704,64]{0,1:T(8,128)(2,1)}, u32[]{:S(2)}) copy-start(bf16[704,64]{0,1:T(8,128)(2,1)} %param.23) | copy-start | bytes 270340
  12.0 13.3 %copy-start.3 = (bf16[384,256]{1,0:T(8,128)(2,1)S(1)}, bf16[384,256]{1,0:T(8,128)(2,1)}, u32[]{:S(2)}) copy-start(bf16[384,256]{1,0:T(8,128)(2,1)} %param.14) | copy-start | bytes 589828
  12.0 186.0 %all-to-all-start = ((bf16[32,384,256]{1,2,0:T(8,128)(2,1)}), bf16[32,384,256]{1,2,0:T(8,128)(2,1)}, u32[]{:S(2)}, u32[]{:S(2)}) async-start(bf16[32,384,256]{1,2,0:T(8,128)(2,1)} %stack.2), calls=%async_computation | async-start | bytes 12582912 | tf_op jit(solution)/shard_map/all_to_all | solution.py:97
  24.3 393.0 %all-gather.5.cloned.1.call-start = ((), (), s32[]{:S(2)}) async-start(), calls=%async_computation.5 | async-start | bytes 9191424 | tf_op jit(solution)/shard_map/all_gather | solution.py:44
  241.3 7.0 %copy-start.1 = (f32[2,2,1536,384]{3,2,1,0:T(8,128)S(1)}, f32[2,2,1536,384]{3,2,1,0:T(8,128)}, u32[]{:S(2)}) copy-start(f32[2,2,1536,384]{3,2,1,0:T(8,128)} %get-tuple-element.149) | copy-start | bytes 28311556 | tf_op jit(solution)/shard_map/while
  257.2 7.2 %copy-start.1 = (f32[2,2,1536,384]{3,2,1,0:T(8,128)S(1)}, f32[2,2,1536,384]{3,2,1,0:T(8,128)}, u32[]{:S(2)}) copy-start(f32[2,2,1536,384]{3,2,1,0:T(8,128)} %get-tuple-element.149) | copy-start | bytes 28311556 | tf_op jit(solution)/shard_map/while
  273.3 7.4 %copy-start.1 = (f32[2,2,1536,384]{3,2,1,0:T(8,128)S(1)}, f32[2,2,1536,384]{3,2,1,0:T(8,128)}, u32[]{:S(2)}) copy-start(f32[2,2,1536,384]{3,2,1,0:T(8,128)} %get-tuple-element.149) | copy-start | bytes 28311556 | tf_op jit(solution)/shard_map/while
  289.7 7.1 %copy-start.1 = (f32[2,2,1536,384]{3,2,1,0:T(8,128)S(1)}, f32[2,2,1536,384]{3,2,1,0:T(8,128)}, u32[]{:S(2)}) copy-start(f32[2,2,1536,384]{3,2,1,0:T(8,128)} %get-tuple-element.149) | copy-start | bytes 28311556 | tf_op jit(solution)/shard_map/while
  305.7 7.0 %copy-start.1 = (f32[2,2,1536,384]{3,2,1,0:T(8,128)S(1)}, f32[2,2,1536,384]{3,2,1,0:T(8,128)}, u32[]{:S(2)}) copy-start(f32[2,2,1536,384]{3,2,1,0:T(8,128)} %get-tuple-element.149) | copy-start | bytes 28311556 | tf_op jit(solution)/shard_map/while
  321.6 7.0 %copy-start.1 = (f32[2,2,1536,384]{3,2,1,0:T(8,128)S(1)}, f32[2,2,1536,384]{3,2,1,0:T(8,128)}, u32[]{:S(2)}) copy-start(f32[2,2,1536,384]{3,2,1,0:T(8,128)} %get-tuple-element.149) | copy-start | bytes 28311556 | tf_op jit(solution)/shard_map/while
  337.5 7.0 %copy-start.1 = (f32[2,2,1536,384]{3,2,1,0:T(8,128)S(1)}, f32[2,2,1536,384]{3,2,1,0:T(8,128)}, u32[]{:S(2)}) copy-start(f32[2,2,1536,384]{3,2,1,0:T(8,128)} %get-tuple-element.149) | copy-start | bytes 28311556 | tf_op jit(solution)/shard_map/while
  353.4 7.0 %copy-start.1 = (f32[2,2,1536,384]{3,2,1,0:T(8,128)S(1)}, f32[2,2,1536,384]{3,2,1,0:T(8,128)}, u32[]{:S(2)}) copy-start(f32[2,2,1536,384]{3,2,1,0:T(8,128)} %get-tuple-element.149) | copy-start | bytes 28311556 | tf_op jit(solution)/shard_map/while
  363.1 0.7 copy-start.8
  363.1 0.8 copy-start.9
  364.7 28.2 %copy-start.2 = (bf16[48,2048]{1,0:T(8,128)(2,1)S(1)}, bf16[48,2048]{1,0:T(8,128)(2,1)}, u32[]{:S(2)}) copy-start(bf16[48,2048]{1,0:T(8,128)(2,1)} %param.13) | copy-start | bytes 589828
  364.7 28.3 %copy-start.7 = (f32[2048]{0:T(1024)S(1)}, f32[2048]{0:T(1024)}, u32[]{:S(2)}) copy-start(f32[2048]{0:T(1024)} %param.20) | copy-start | bytes 24580
Sparse Core Ops, SparseCore 0:
  9.9 180.8 all-gather.2
  193.4 108.8 all-gather.4
